TPU v7x, 32 devices: a whole 2x2x4 slice. The times are simulated.
32 devices in a mesh: fs: 8 (over z, x), tp: 4 (over y, core).
Axes of the slice: x: 2, y: 2, z: 4, core: 2. Of those that a mesh axis runs over, the one named last changes fastest.
Arguments:
- h_saved: bfloat16 [16384, 2048], P('fs'), may hold values from -6 to 6
- conv_cotan: bfloat16 [16384, 2560], P('fs', 'tp'), may hold values from -64 to 64
- lru_out: bfloat16 [16384, 2560], P('fs', 'tp'), may hold values from -64 to 64
- out_cotan: bfloat16 [16384, 2048], P('fs'), may hold values from -6 to 6
- basis_in: bfloat16 [2048, 256], P('fs'), may hold values from -1.41421356 to 1.41421356
- basis_out: bfloat16 [2048, 256], P('fs'), may hold values from -1.41421356 to 1.41421356
- weight_in: float32 [2048, 2560], P('fs', 'tp'), may hold values from -0.125 to 0.125
- weight_out: float32 [2560, 2048], P('tp', 'fs'), may hold values from -0.125 to 0.125
- first_in: float32 [256, 2560], P('fs', 'tp'), may hold values from -6 to 6
- second_in: float32 [256, 2560], P('fs', 'tp'), may hold values from 0.05 to 2
- first_out: float32 [256, 2560], P('fs', 'tp'), may hold values from -6 to 6
- second_out: float32 [256, 2560], P('fs', 'tp'), may hold values from 0.05 to 2
Outputs:
- step_in: float32 [2048, 2560], P('fs', 'tp')
- new_weight_in: float32 [2048, 2560], P('fs', 'tp')
- copy_in: bfloat16 [2048, 2560], P(None, 'tp')
- new_first_in: float32 [256, 2560], P('fs', 'tp')
- new_second_in: float32 [256, 2560], P('fs', 'tp')
- step_out: float32 [2560, 2048], P('tp', 'fs')
- new_weight_out: float32 [2560, 2048], P('tp', 'fs')
- copy_out: bfloat16 [2560, 2048], P('tp')
- new_first_out: float32 [256, 2560], P('fs', 'tp')
- new_second_out: float32 [256, 2560], P('fs', 'tp')
All inputs are finite; a program needn't handle non-finite values.
Results may differ from a plain program's by a relative error of at most 0.0046.
Values may be sent and summed in bfloat16 or wider, within the bound.
A program may use at most 128 MiB of HBM per device.

v0:
```python
import math

import jax
import jax.numpy as jnp
from jax import lax
from jax.sharding import PartitionSpec as P

D_RNN = 2560
RANK = 256


def split_product(narrow, wide):
    upper = lax.optimization_barrier(wide.astype(jnp.bfloat16))
    lower = (wide - upper.astype(jnp.float32)).astype(jnp.bfloat16)
    turned = jnp.transpose(narrow)
    first_part = jnp.dot(turned, upper, preferred_element_type=jnp.float32)
    second_part = jnp.dot(turned, lower, preferred_element_type=jnp.float32)
    return first_part + second_part


def moments(proj, factor, first, second):
    scaled = factor * proj
    first_new = 0.8 * first + 0.2 * scaled
    second_new = 0.9 * second + 0.1 * scaled * scaled
    direction = (first_new / (jnp.sqrt(second_new) + 1e-08)).astype(jnp.bfloat16)
    return (first_new, second_new, direction)


def shards(
    h_saved,
    conv_cotan,
    lru_out,
    out_cotan,
    basis_in,
    basis_out,
    weight_in,
    weight_out,
    first_in,
    second_in,
    first_out,
    second_out,
):
    pairs = ((h_saved, conv_cotan), (out_cotan, lru_out))
    partial_value = []
    wholes = (
        lax.all_gather(basis_in, "fs", axis=0, tiled=True),
        lax.all_gather(basis_out, "fs", axis=0, tiled=True),
    )
    for number in range(2):
        reduced = jnp.dot(pairs[number][0], wholes[number], preferred_element_type=jnp.float32)
        partial_value.append(split_product(pairs[number][1], reduced).T)
    proj_in, proj_out = (
        lax.psum_scatter(partial_value[0], "fs", scatter_dimension=0, tiled=True),
        lax.psum_scatter(partial_value[1], "fs", scatter_dimension=0, tiled=True),
    )
    total = lax.psum(jnp.sum(proj_in * proj_in) + jnp.sum(proj_out * proj_out), ("fs", "tp"))
    factor = math.sqrt(2.0 * RANK * D_RNN) * lax.rsqrt(total + 1e-06)
    first_a, second_a, dir_in = moments(proj_in, factor, first_in, second_in)
    first_b, second_b, dir_out = moments(proj_out, factor, first_out, second_out)
    full_in, full_out = (
        lax.all_gather(dir_in, "fs", axis=0, tiled=True),
        lax.all_gather(dir_out, "fs", axis=0, tiled=True),
    )
    step_in = jnp.dot(basis_in, full_in, preferred_element_type=jnp.float32)
    step_out = jnp.dot(basis_out, full_out, preferred_element_type=jnp.float32).T
    new_in = weight_in - 0.02 * step_in
    new_out = weight_out - 0.02 * step_out
    copy_in, copy_out = (
        lax.all_gather(new_in.astype(jnp.bfloat16), "fs", axis=0, tiled=True),
        lax.all_gather(new_out.astype(jnp.bfloat16), "fs", axis=1, tiled=True),
    )
    return (
        step_in,
        new_in,
        copy_in,
        first_a,
        second_a,
        step_out,
        new_out,
        copy_out,
        first_b,
        second_b,
    )


def solution(mesh):
    return jax.shard_map(
        shards,
        mesh=mesh,
        in_specs=(
            P("fs", None),
            P("fs", "tp"),
            P("fs", "tp"),
            P("fs", None),
            P("fs", None),
            P("fs", None),
            P("fs", "tp"),
            P("tp", "fs"),
            P("fs", "tp"),
            P("fs", "tp"),
            P("fs", "tp"),
            P("fs", "tp"),
        ),
        out_specs=(
            P("fs", "tp"),
            P("fs", "tp"),
            P(None, "tp"),
            P("fs", "tp"),
            P("fs", "tp"),
            P("tp", "fs"),
            P("tp", "fs"),
            P("tp", None),
            P("fs", "tp"),
            P("fs", "tp"),
        ),
        check_vma=False,
    )
```

profile of v0, /device:TPU:0, one launch (start us, length us, event | category | flops | bytes accessed | tf_op | source)
XLA Modules:
  0.0 430.1 jit_solution(16301647200006217187)
XLA Ops:
  7.2 0.0 copy-start
  7.2 0.0 all-gather.7.cloned.1.call-start
  7.2 0.7 all-gather.7.cloned.1.call-update
  7.9 0.0 all-gather.5.cloned.1.call-start
  8.0 0.7 all-gather.5.cloned.1.call-update
  8.7 0.0 reduce-scatter.5.cloned.1.call-start
  8.7 44.4 %all-gather.7.cloned.1.call-done = bf16[2048,256]{1,0:T(8,128)(2,1)} async-done(((bf16[256,256]{1,0:T(8,128)(2,1)}), bf16[2048,256]{1,0:T(8,128)(2,1)}) %all-gather.7.cloned.1.call-update) | async-done | bytes 1048592 | tf_op jit(solution)/shard_map/all_gather | solution.py:47
  53.2 6.1 %fusion.7 = (bf16[2048,256]{1,0:T(8,128)(2,1)S(1)}, f32[2048,256]{1,0:T(8,128)S(1)}) fusion(bf16[2048,2048]{1,0:T(8,128)(2,1)} %param.15, bf16[2048,256]{1,0:T(8,128)(2,1)} %all-gather.7.cloned.1.call-done), kind=kOutput, calls=%fused_computation.20 | convolution fusion | flops 2148007936 | bytes 12582912 | tf_op jit(solution)/shard_map/dot_general | solution.py:50
  59.2 0.0 copy-done
  59.2 1.0 fusion.9
  60.3 1.9 convolution_add_fusion
  62.2 0.0 reduce-scatter.5.cloned.1.call-update
  62.2 0.0 reduce-scatter.3.cloned.1.call-start
  62.3 32.0 %all-gather.5.cloned.1.call-done = bf16[2048,256]{1,0:T(8,128)(2,1)} async-done(((bf16[256,256]{1,0:T(8,128)(2,1)}), bf16[2048,256]{1,0:T(8,128)(2,1)}) %all-gather.5.cloned.1.call-update) | async-done | bytes 1048592 | tf_op jit(solution)/shard_map/all_gather | solution.py:46
  94.3 0.0 copy-start.1
  94.3 6.2 %fusion.6 = (bf16[2048,256]{1,0:T(8,128)(2,1)S(1)}, f32[2048,256]{1,0:T(8,128)S(1)}) fusion(bf16[2048,2048]{1,0:T(8,128)(2,1)} %param.12, bf16[2048,256]{1,0:T(8,128)(2,1)} %all-gather.5.cloned.1.call-done), kind=kOutput, calls=%fused_computation.19 | convolution fusion | flops 2148007936 | bytes 12582912 | tf_op jit(solution)/shard_map/dot_general | solution.py:50
  100.5 0.0 copy-done.1
  100.5 1.0 fusion.8
  101.6 0.0 copy-start.2
  101.6 1.9 convolution_add_fusion.1
  103.5 0.0 copy-start.3
  103.5 0.0 reduce-scatter.3.cloned.1.call-update
  103.5 0.0 all-gather.9.cloned.1.call-start
  103.5 56.1 %reduce-scatter.5.cloned.1.call-done = f32[32,640]{1,0:T(8,128)} async-done(((f32[256,640]{1,0:T(8,128)}), f32[32,640]{1,0:T(8,128)}) %reduce-scatter.5.cloned.1.call-update) | async-done | bytes 81936 | tf_op jit(solution)/shard_map/reduce_scatter | solution.py:54
  159.7 1.5 multiply_reduce_fusion
  161.2 64.0 %reduce-scatter.3.cloned.1.call-done = f32[32,640]{1,0:T(8,128)} async-done(((f32[256,640]{1,0:T(8,128)}), f32[32,640]{1,0:T(8,128)}) %reduce-scatter.3.cloned.1.call-update) | async-done | bytes 81936 | tf_op jit(solution)/shard_map/reduce_scatter | solution.py:53
  225.2 1.5 multiply_reduce_fusion.1
  228.0 0.0 copy-done.2
  228.0 1.1 copy.22
  229.1 0.0 copy-start.4
  229.1 39.8 %psum.7 = f32[]{:T(128)} all-reduce(f32[]{:T(128)S(6)} %add.40), channel_id=1, replica_groups=mesh['fs'=8,'tp'=4] {'fs','tp'}, use_global_device_ids=true, to_apply=%region_4.0 | all-reduce | flops 1 | bytes 8 | tf_op jit(solution)/shard_map/psum | solution.py:56
  269.6 1.7 divide_convert_fusion.1
  271.2 30.8 %all_gather.20 = bf16[256,640]{1,0:T(8,128)(2,1)S(1)} all-gather(bf16[32,640]{1,0:T(8,128)(2,1)S(1)} %get-tuple-element.27), channel_id=1, replica_groups=mesh['fs'=8,'tp'=4] {'fs'}, dimensions={0}, use_global_device_ids=true | all-gather | bytes 368640 | tf_op jit(solution)/shard_map/all_gather | solution.py:61
  302.1 0.0 copy-done.3
  302.1 2.3 fusion.4
  304.4 0.0 all-gather.9.cloned.1.call-update
  304.5 0.0 all-gather.11.cloned.1.call-start
  304.5 1.7 divide_convert_fusion
  306.2 31.9 %all_gather.22 = bf16[256,640]{1,0:T(8,128)(2,1)S(1)} all-gather(bf16[32,640]{1,0:T(8,128)(2,1)S(1)} %get-tuple-element.22), channel_id=1, replica_groups=mesh['fs'=8,'tp'=4] {'fs'}, dimensions={0}, use_global_device_ids=true | all-gather | bytes 368640 | tf_op jit(solution)/shard_map/all_gather | solution.py:62
  338.1 0.0 copy-done.4
  338.1 2.6 fusion.2
  340.6 0.0 all-gather.11.cloned.1.call-update
  340.7 2.2 copy.24
  342.8 1.1 copy.23
  343.9 18.1 %all-gather.9.cloned.1.call-done = bf16[2048,640]{0,1:T(8,128)(2,1)} async-done(((bf16[256,640]{0,1:T(8,128)(2,1)}), bf16[2048,640]{0,1:T(8,128)(2,1)}) %all-gather.9.cloned.1.call-update) | async-done | bytes 2621456 | tf_op jit(solution)/shard_map/all_gather | solution.py:69
  362.0 4.4 %copy.25 = bf16[2048,640]{1,0:T(8,128)(2,1)} copy(bf16[2048,640]{0,1:T(8,128)(2,1)} %all-gather.9.cloned.1.call-done) | data formatting | bytes 5242880
  366.4 53.3 %all-gather.11.cloned.1.call-done = bf16[640,2048]{1,0:T(8,128)(2,1)} async-done(((bf16[640,256]{1,0:T(8,128)(2,1)}), bf16[640,2048]{1,0:T(8,128)(2,1)}) %all-gather.11.cloned.1.call-update) | async-done | bytes 2621456 | tf_op jit(solution)/shard_map/all_gather | solution.py:70
  419.7 3.6 copy.27
Async XLA Ops:
  7.2 52.1 %copy-start = (bf16[2048,640]{1,0:T(8,128)(2,1)S(1)}, bf16[2048,640]{1,0:T(8,128)(2,1)}, u32[]{:S(2)}) copy-start(bf16[2048,640]{1,0:T(8,128)(2,1)} %param.14) | copy-start | bytes 7864324
  7.2 46.0 %all-gather.7.cloned.1.call-start = ((), (), s32[]{:S(2)}) async-start(), calls=%async_computation.4 | async-start | bytes 1179648 | tf_op jit(solution)/shard_map/all_gather | solution.py:47
  7.9 86.4 %all-gather.5.cloned.1.call-start = ((), (), s32[]{:S(2)}) async-start(), calls=%async_computation.2 | async-start | bytes 1179648 | tf_op jit(solution)/shard_map/all_gather | solution.py:46
  8.7 151.0 %reduce-scatter.5.cloned.1.call-start = ((), (), s32[]{:S(2)}) async-start(), calls=%async_computation.5 | async-start | bytes 737280 | tf_op jit(solution)/shard_map/reduce_scatter | solution.py:54
  62.2 162.9 %reduce-scatter.3.cloned.1.call-start = ((), (), s32[]{:S(2)}) async-start(), calls=%async_computation.3 | async-start | bytes 737280 | tf_op jit(solution)/shard_map/reduce_scatter | solution.py:53
  94.3 6.2 %copy-start.1 = (bf16[2048,640]{1,0:T(8,128)(2,1)S(1)}, bf16[2048,640]{1,0:T(8,128)(2,1)}, u32[]{:S(2)}) copy-start(bf16[2048,640]{1,0:T(8,128)(2,1)} %param.13) | copy-start | bytes 7864324
  101.6 126.4 %copy-start.2 = (f32[256,640]{1,0:T(8,128)S(1)}, f32[256,640]{1,0:T(8,128)}, u32[]{:S(2)}) copy-start(f32[256,640]{1,0:T(8,128)} %param.18) | copy-start | bytes 1966084
  103.5 198.6 %copy-start.3 = (bf16[256,256]{1,0:T(8,128)(2,1)S(1)}, bf16[256,256]{1,0:T(8,128)(2,1)}, u32[]{:S(2)}) copy-start(bf16[256,256]{1,0:T(8,128)(2,1)} %param.16) | copy-start | bytes 393220
  103.5 258.5 %all-gather.9.cloned.1.call-start = ((), (), s32[]{:S(2)}) async-start(), calls=%async_computation.6 | async-start | bytes 2949120 | tf_op jit(solution)/shard_map/all_gather | solution.py:69
  229.1 109.0 %copy-start.4 = (bf16[256,256]{1,0:T(8,128)(2,1)S(1)}, bf16[256,256]{1,0:T(8,128)(2,1)}, u32[]{:S(2)}) copy-start(bf16[256,256]{1,0:T(8,128)(2,1)} %param.17) | copy-start | bytes 393220
  304.5 115.2 %all-gather.11.cloned.1.call-start = ((), (), s32[]{:S(2)}) async-start(), calls=%async_computation.7 | async-start | bytes 2949120 | tf_op jit(solution)/shard_map/all_gather | solution.py:70
Sparse Core Ops, SparseCore 0:
  10.1 42.9 all-gather.6
  55.3 38.9 all-gather.4
  98.2 61.4 reduce-scatter.4
  163.4 61.7 reduce-scatter.2
  304.6 57.3 all-gather.8
  363.9 55.7 all-gather.10
where the time goes:
time: 431 us; the launch traced here: 430 us
  waiting for transfers between devices  269 us (62%)
  blocking collectives  103 us (24%)
  matrix products  23.1 us (5%)
  between operations  16.2 us (4%)
  local copies, waits for them, and re-layouts  12.3 us (3%)
  other arithmetic  6.38 us (1%)
    reduce_scatter x1, waiting for transfers between devices, shards(): lax.psum_scatter(partial_value[0], 'fs', scatter_dimension=0, tiled=True)  64 us
    reduce_scatter x1, waiting for transfers between devices, shards(): lax.psum_scatter(partial_value[1], 'fs', scatter_dimension=0, tiled=True)  56.1 us
    all_gather x1, waiting for transfers between devices, shards(): lax.all_gather(new_out.astype(jnp.bfloat16), 'fs', axis=1, tiled=True)  53.3 us
    all_gather x1, waiting for transfers between devices, shards(): lax.all_gather(basis_out, 'fs', axis=0, tiled=True)  44.4 us
    psum x1, blocking collectives, shards(): lax.psum(jnp.sum(proj_in * proj_in) + jnp.sum(proj_out * proj_out), ('fs'...  39.8 us
    all_gather x1, waiting for transfers between devices, shards(): lax.all_gather(basis_in, 'fs', axis=0, tiled=True)  32 us
    all_gather x1, blocking collectives, shards(): lax.all_gather(dir_out, 'fs', axis=0, tiled=True)  31.9 us
    all_gather x1, blocking collectives, shards(): lax.all_gather(dir_in, 'fs', axis=0, tiled=True)  30.8 us
  transfers between devices with their start and end apart: 6, of which 6 were waited for; matrix products, arithmetic and copies ran while one was open for 7% of the time, Pallas kernels for 0%

commit v1 on v0

v1 whole, which is shorter than its diff:
```python
import functools
import math

import jax
import jax.numpy as jnp
from jax import lax
from jax.experimental import pallas as pl
from jax.experimental.pallas import tpu as pltpu
from jax.sharding import PartitionSpec as P

MESH = pl.DeviceIdType.MESH
VMEM_LIMIT = 60 * 1024 * 1024


def nt_dot(left, right):
    return lax.dot_general(left, right, (((1,), (1,)), ((), ())), preferred_element_type=jnp.float32)


def exchange(
    dims,
    h_hbm,
    cc_hbm,
    oc_hbm,
    lo_hbm,
    basis_in,
    basis_out,
    w_in,
    w_out,
    m_in,
    v_in,
    m_out,
    v_out,
    ball,
    win_all,
    wout_all,
    dall,
    nm_in,
    nv_in,
    nm_out,
    nv_out,
    h_buf,
    c_buf,
    acc,
    part,
    part_in,
    tot,
    tot_in,
    in_sem,
    ss,
    rs,
    cs,
    cr,
    ps,
    pr,
    ts,
    tr,
):
    F, T, Z, X, scale = dims
    f = lax.axis_index("fs")
    t = lax.axis_index("tp")
    z, x = f // X, f % X
    core = t % 2
    mate = t + 1 - 2 * core
    tokens, chunk = h_buf.shape[1], h_buf.shape[1] // in_sem.shape[1]
    chunks = in_sem.shape[1]
    rr = m_in.shape[0]

    def fetch(which, i):
        rows = pl.ds(i * chunk, chunk)
        h_src, c_src = ((h_hbm, cc_hbm), (oc_hbm, lo_hbm))[which]
        return (
            pltpu.make_async_copy(h_src.at[rows], h_buf.at[which, rows], in_sem.at[which, i, 0]),
            pltpu.make_async_copy(c_src.at[rows], c_buf.at[which, rows], in_sem.at[which, i, 1]),
        )

    for which in range(2):
        for i in range(chunks):
            for copy in fetch(which, i):
                copy.start()

    barrier = pltpu.get_barrier_semaphore()

    def greet(n, carry):
        pl.semaphore_signal(
            barrier, inc=1, device_id=((f + n // T) % F, (t + n % T) % T), device_id_type=MESH
        )
        return carry

    lax.fori_loop(1, F * T, greet, 0)
    for which, basis in enumerate((basis_in, basis_out)):
        ball[which, f] = basis[...]
    win_all[f] = w_in[...].astype(jnp.bfloat16)
    wout_all[f] = w_out[...].astype(jnp.bfloat16)
    pl.semaphore_wait(barrier, F * T - 1)

    def source(k, j):
        return ((z + Z - k) % Z) * X + (x + X - j) % X

    half = basis_in.shape[0] // 2
    q_in, q_out = w_in.shape[0] // 2, w_out.shape[0] // 2

    def place(item, s, core):
        if item < 2:
            return ball.at[item, s, pl.ds(pl.multiple_of(core * half, half), half)]
        if item < 4:
            return win_all.at[s, pl.ds((item - 2) * q_in, q_in)]
        if item < 6:
            return wout_all.at[s, pl.ds((item - 4) * q_out, q_out)]
        return dall.at[item - 6, s]

    def own(item):
        if item < 2:
            return (basis_in, basis_out)[item].at[pl.ds(pl.multiple_of(core * half, half), half)]
        return place(item, f, core)

    def along_z(item, k, src=None):
        at = place(item, f, core)
        return pltpu.make_async_remote_copy(
            src_ref=at if src is None else src,
            dst_ref=at,
            send_sem=ss.at[item, k, 0],
            recv_sem=rs.at[item, k, 0],
            device_id=(((z + k) % Z) * X + x, t),
            device_id_type=MESH,
        )

    def along_x(item, k, j, src=None):
        at = place(item, source(k, 0), core)
        return pltpu.make_async_remote_copy(
            src_ref=at if src is None else src,
            dst_ref=at,
            send_sem=ss.at[item, k, j],
            recv_sem=rs.at[item, k, j],
            device_id=(z * X + (x + j) % X, t),
            device_id_type=MESH,
        )

    def across(item, k, j, side=None):
        at = place(item, source(k, j), core if side is None else side)
        return pltpu.make_async_remote_copy(
            src_ref=at,
            dst_ref=at,
            send_sem=cs.at[item, k, j],
            recv_sem=cr.at[item, k, j],
            device_id=(f, mate),
            device_id_type=MESH,
        )

    def arrived(item, k, j):
        at = place(item, source(k, j), core)
        pltpu.make_async_remote_copy(
            src_ref=at,
            dst_ref=at,
            send_sem=ss.at[item, k, j],
            recv_sem=rs.at[item, k, j],
            device_id=((f + 1) % F, t),
            device_id_type=MESH,
        ).wait_recv()

    def begin(item):
        src = own(item)
        for k in range(1, Z):
            along_z(item, k, src).start()
        for j in range(1, X):
            along_x(item, 0, j, src).start()

    def forward(item):
        for k in range(1, Z):
            arrived(item, k, 0)
            for j in range(1, X):
                along_x(item, k, j).start()
            if item < 2:
                across(item, k, 0).start()

    def finish(item):
        for k in range(Z):
            for j in range(1, X):
                arrived(item, k, j)
                if item < 2:
                    across(item, k, j).start()
        if item < 2:
            for k in range(Z):
                for j in range(X):
                    if k or j:
                        across(item, k, j, 1 - core).wait_recv()

    def drain(item):
        for k in range(Z):
            for j in range(X):
                if j:
                    along_x(item, k, j).wait_send()
                elif k:
                    along_z(item, k).wait_send()
                if item < 2 and (k or j):
                    across(item, k, j).wait_send()

    def project(which):
        acc[which] = jnp.zeros(acc.shape[1:], jnp.float32)

        def step(i, carry):
            for copy in fetch(which, i):
                copy.wait()
            rows = pl.ds(pl.multiple_of(i * chunk, chunk), chunk)
            whole = ball[which].reshape(h_buf.shape[2], -1)
            reduced = jnp.dot(h_buf[which, rows], whole, preferred_element_type=jnp.float32)
            turned = reduced.T
            upper = turned.astype(jnp.bfloat16)
            lower = (turned - upper.astype(jnp.float32)).astype(jnp.bfloat16)
            block = c_buf[which, rows]
            acc[which] += jnp.dot(upper, block, preferred_element_type=jnp.float32) + jnp.dot(
                lower, block, preferred_element_type=jnp.float32
            )
            return carry

        lax.fori_loop(0, chunks, step, 0)
        part[which] = acc[which].astype(jnp.bfloat16).reshape(part.shape[1:])

    def scatter(which, d):
        peer = (f + d) % F
        return pltpu.make_async_remote_copy(
            src_ref=part.at[which, peer],
            dst_ref=part_in.at[which, d],
            send_sem=ps.at[which, d],
            recv_sem=pr.at[which, d],
            device_id=(peer, t),
            device_id_type=MESH,
        )

    def share(n):
        return pltpu.make_async_remote_copy(
            src_ref=tot,
            dst_ref=tot_in.at[n],
            send_sem=ts.at[n],
            recv_sem=tr.at[n],
            device_id=((f + n // T) % F, (t + n % T) % T),
            device_id_type=MESH,
        )

    begin(0)
    begin(1)
    forward(0)
    forward(1)
    begin(2)
    finish(0)
    project(0)
    for d in range(1, F):
        scatter(0, d).start()
    finish(1)
    project(1)
    for d in range(1, F):
        scatter(1, d).start()
    forward(2)
    begin(3)
    projs = []
    square = jnp.zeros((1, 1), jnp.float32)
    for which in range(2):
        value = acc[which, pl.ds(pl.multiple_of(f * rr, rr), rr)]
        for d in range(1, F):
            scatter(which, d).wait_recv()
            value = value + part_in[which, d].astype(jnp.float32)
        projs.append(value)
        square = square + jnp.sum(value * value, axis=(0, 1), keepdims=True)
    tot[...] = jnp.broadcast_to(square, tot.shape)
    tot_in[0] = tot[...]

    def share_start(n, carry):
        share(n).start()
        return carry

    def share_wait(n, carry):
        share(n).wait()
        return carry

    lax.fori_loop(1, F * T, share_start, 0)
    lax.fori_loop(1, F * T, share_wait, 0)
    total = jnp.sum(tot_in[...], axis=0)
    factor = (scale * lax.rsqrt(total + 1e-06))[0:1, 0:1]
    for which, (first, second, first_to, second_to) in enumerate(
        ((m_in, v_in, nm_in, nv_in), (m_out, v_out, nm_out, nv_out))
    ):
        scaled = factor * projs[which]
        first_new = 0.8 * first[...] + 0.2 * scaled
        second_new = 0.9 * second[...] + 0.1 * scaled * scaled
        first_to[...] = first_new
        second_to[...] = second_new
        dall[which, f] = (first_new / (jnp.sqrt(second_new) + 1e-08)).astype(jnp.bfloat16)
    begin(6)
    begin(7)
    begin(4)
    begin(5)
    forward(3)
    forward(6)
    forward(7)
    forward(4)
    forward(5)
    for item in (2, 3, 6, 7, 4, 5):
        finish(item)
    for item in range(8):
        drain(item)
    for which in range(2):
        for d in range(1, F):
            scatter(which, d).wait_send()


def apply_step(
    basis_in, basis_out, w_in, w_out, nm_in, nv_in, nm_out, nv_out, b_in, b_out, win, wout, dirs,
    step_in, new_in, copy_in, o_m_in, o_v_in, step_out, new_out, copy_out, o_m_out, o_v_out, turned,
):
    direction = dirs[0].reshape(-1, dirs.shape[3])

    @pl.when(pl.program_id(0) == 0)
    def _():
        other = dirs[1].reshape(-1, dirs.shape[3])
        turned[...] = other.astype(jnp.float32).T.astype(jnp.bfloat16)
        for source, target in ((nm_in, o_m_in), (nv_in, o_v_in), (nm_out, o_m_out), (nv_out, o_v_out)):
            target[...] = source[...]
        step = jnp.dot(basis_in[...], direction, preferred_element_type=jnp.float32)
        step_in[...] = step
        new_in[...] = w_in[...] - 0.02 * step
        step = nt_dot(turned[...], basis_out[...])
        step_out[...] = step
        new_out[...] = w_out[...] - 0.02 * step

    step = jnp.dot(b_in[0, 0], direction, preferred_element_type=jnp.float32)
    copy_in[...] = (win[0].astype(jnp.float32) - 0.02 * step).astype(jnp.bfloat16)
    step = nt_dot(turned[...], b_out[0, 0])
    copy_out[...] = (wout[0].astype(jnp.float32) - 0.02 * step).astype(jnp.bfloat16)


def shards(mesh, h, cc, lo, oc, basis_in, basis_out, w_in, w_out, m_in, v_in, m_out, v_out):
    F, T = mesh.shape["fs"], mesh.shape["tp"]
    Z = next(n for n in range(1, F + 1) if F % n == 0 and n * n >= F)
    X = F // Z
    tokens, model = h.shape
    cols = cc.shape[1]
    rows, rank = basis_in.shape
    rr = m_in.shape[0]
    scale = math.sqrt(2.0 * rank * cols * T)
    chunks = max(1, tokens // 512)
    bf, f32 = jnp.bfloat16, jnp.float32
    hbm = pl.BlockSpec(memory_space=pl.ANY)
    vmem = pl.BlockSpec(memory_space=pltpu.VMEM)
    moment = jax.ShapeDtypeStruct(m_in.shape, f32)
    dma = pltpu.SemaphoreType.DMA
    ball, win_all, wout_all, dall, *moments = pl.pallas_call(
        functools.partial(exchange, (F, T, Z, X, scale)),
        out_shape=(
            jax.ShapeDtypeStruct((2, F, rows, rank), bf),
            jax.ShapeDtypeStruct((F,) + w_in.shape, bf),
            jax.ShapeDtypeStruct((F,) + w_out.shape, bf),
            jax.ShapeDtypeStruct((2, F, rr, cols), bf),
            moment,
            moment,
            moment,
            moment,
        ),
        in_specs=[hbm] * 4 + [vmem] * 8,
        out_specs=(vmem,) * 8,
        scratch_shapes=[
            pltpu.VMEM((2, tokens, model), bf),
            pltpu.VMEM((2, tokens, cols), bf),
            pltpu.VMEM((2, rank, cols), f32),
            pltpu.VMEM((2, F, rr, cols), bf),
            pltpu.VMEM((2, F, rr, cols), bf),
            pltpu.VMEM((8, 128), f32),
            pltpu.VMEM((F * T, 8, 128), f32),
            dma((2, chunks, 2)),
            dma((8, Z, X)),
            dma((8, Z, X)),
            dma((2, Z, X)),
            dma((2, Z, X)),
            dma((2, F)),
            dma((2, F)),
            dma((F * T,)),
            dma((F * T,)),
        ],
        compiler_params=pltpu.CompilerParams(
            collective_id=0, has_side_effects=True, vmem_limit_bytes=VMEM_LIMIT
        ),
        name="exchange",
    )(h, cc, oc, lo, basis_in, basis_out, w_in, w_out, m_in, v_in, m_out, v_out)

    def fixed(array):
        return pl.BlockSpec(array.shape, lambda i, n=array.ndim: (0,) * n)

    keep = (basis_in, basis_out, w_in, w_out, *moments)
    outs = (
        (w_in.shape, f32, None),
        (w_in.shape, f32, None),
        ((model, cols), bf, pl.BlockSpec(w_in.shape, lambda i: (i, 0))),
        (m_in.shape, f32, None),
        (m_in.shape, f32, None),
        (w_out.shape, f32, None),
        (w_out.shape, f32, None),
        ((cols, model), bf, pl.BlockSpec(w_out.shape, lambda i: (0, i))),
        (m_in.shape, f32, None),
        (m_in.shape, f32, None),
    )
    return pl.pallas_call(
        apply_step,
        grid=(F,),
        out_shape=tuple(jax.ShapeDtypeStruct(shape, kind) for shape, kind, _ in outs),
        in_specs=[fixed(a) for a in keep]
        + [
            pl.BlockSpec((1, 1, rows, rank), lambda i: (0, i, 0, 0)),
            pl.BlockSpec((1, 1, rows, rank), lambda i: (1, i, 0, 0)),
            pl.BlockSpec((1,) + w_in.shape, lambda i: (i, 0, 0)),
            pl.BlockSpec((1,) + w_out.shape, lambda i: (i, 0, 0)),
            fixed(dall),
        ],
        out_specs=tuple(
            spec or pl.BlockSpec(shape, lambda i, n=len(shape): (0,) * n) for shape, _, spec in outs
        ),
        scratch_shapes=[pltpu.VMEM((cols, rank), bf)],
        compiler_params=pltpu.CompilerParams(vmem_limit_bytes=VMEM_LIMIT),
        name="apply_step",
    )(*keep, ball, ball, win_all, wout_all, dall)


def solution(mesh):
    split, both = P("fs", None), P("fs", "tp")
    return jax.shard_map(
        functools.partial(shards, mesh),
        mesh=mesh,
        in_specs=(split, both, both, split, split, split, both, P("tp", "fs"), both, both, both, both),
        out_specs=(both, both, P(None, "tp"), both, both, P("tp", "fs"), P("tp", "fs"), P("tp", None), both, both),
        check_vma=False,
    )
```

time: 431 us -> 132 us (0.31)
  waiting for transfers between devices: 269 us -> 0 us
  Pallas kernels: 0 us -> 131 us
  blocking collectives: 103 us -> 0 us
  matrix products: 23.1 us -> 0 us
  between operations: 16.2 us -> 0.65 us
  local copies, waits for them, and re-layouts: 12.3 us -> 0 us
  other arithmetic: 6.38 us -> 0 us
    all_gather x4 -> x0, waiting for transfers between devices: 148 us -> none  [the longest x1 53.3 us: shards(): lax.all_gather(new_out.astype(jnp.bfloat16), 'fs', axis=1, tiled=True)]
    pallas_call x0 -> x2, Pallas kernels: none -> 131 us  [the longest x1 121 us: shards(): pl.pallas_call(functools.partial(exchange, (F, T, Z, X, scale)), out_shap...]
    reduce_scatter x2 -> x0, waiting for transfers between devices: 120 us -> none  [the longest x1 64 us: shards(): lax.psum_scatter(partial_value[0], 'fs', scatter_dimension=0, tiled=True)]
    all_gather x2 -> x0, blocking collectives: 62.7 us -> none  [the longest x1 31.9 us: shards(): lax.all_gather(dir_out, 'fs', axis=0, tiled=True)]
    psum x1 -> x0, blocking collectives: 39.8 us -> none  [shards(): lax.psum(jnp.sum(proj_in * proj_in) + jnp.sum(proj_out * proj_out), ('fs'...]
    dot_general x8 -> x0, matrix products: 23.1 us -> none  [the longest x2 12.3 us: shards(): jnp.dot(pairs[number][0], wholes[number], preferred_element_type=jnp.floa...]
    unnamed x15 -> x0, local copies, waits for them, and re-layouts: 12.3 us -> none
  transfers between devices with their start and end apart: 6 -> 0, of which waited for: 6 -> 0; matrix products, arithmetic and copies ran while one was open for 7% -> 0% of each run, Pallas kernels for 0% -> 0%
where the time goes in v1:
time: 132 us
  Pallas kernels  131 us (99%)
    pallas_call x1, Pallas kernels, shards(): pl.pallas_call(functools.partial(exchange, (F, T, Z, X, scale)), out_shap...  121 us
    pallas_call x1, Pallas kernels, shards(): pl.pallas_call(apply_step, grid=(F,), out_shape=tuple((jax.ShapeDtypeStru...  10.8 us

profile of v1, /device:TPU:0, one launch (start us, length us, event | category | flops | bytes accessed | tf_op | source)
XLA Modules:
  0.0 132.1 jit_solution(4829080011706269045)
XLA Ops:
  0.6 120.6 %exchange.1 = (bf16[2,8,256,256]{3,2,1,0:T(8,128)(2,1)}, bf16[8,256,640]{2,1,0:T(8,128)(2,1)}, bf16[8,640,256]{2,1,0:T(8,128)(2,1)}, bf16[2,8,32,640]{3,2,1,0:T(...) custom-call(bf16[2048,2048]{1,0:T(8,128)(2,1)} %h_hbm.1, ...), custom_call_target="tpu_custom_call" | custom-call | tf_op jit(solution)/shard_map/exchange/pallas_call | solution.py:345
  121.3 10.8 %apply_step.1 = (f32[256,640]{1,0:T(8,128)}, f32[256,640]{1,0:T(8,128)}, bf16[2048,640]{1,0:T(8,128)(2,1)}, f32[32,640]{1,0:T(8,128)}, f32[32,640]{1,0:T(8,128)}...) custom-call(bf16[256,256]{1,0:T(8,128)(2,1)} %basis_in.3, ...), custom_call_target="tpu_custom_call" | custom-call | tf_op jit(solution)/shard_map/apply_step/pallas_call | solution.py:399

commit v2 on v1

--- a/solution.py
+++ b/solution.py
@@ -44,6 +44,7 @@
     part,
     part_in,
     tot,
+    tot_two,
     tot_in,
     in_sem,
     ss,
@@ -232,7 +233,17 @@
             dst_ref=tot_in.at[n],
             send_sem=ts.at[n],
             recv_sem=tr.at[n],
-            device_id=((f + n // T) % F, (t + n % T) % T),
+            device_id=(f, (t + n) % T),
+            device_id_type=MESH,
+        )
+
+    def share_on(d):
+        return pltpu.make_async_remote_copy(
+            src_ref=tot_two,
+            dst_ref=tot_in.at[T + d],
+            send_sem=ts.at[T + d],
+            recv_sem=tr.at[T + d],
+            device_id=((f + d) % F, t),
             device_id_type=MESH,
         )
 
@@ -263,17 +274,17 @@
     tot[...] = jnp.broadcast_to(square, tot.shape)
     tot_in[0] = tot[...]
 
-    def share_start(n, carry):
+    for n in range(1, T):
         share(n).start()
-        return carry
-
-    def share_wait(n, carry):
+    for n in range(1, T):
         share(n).wait()
-        return carry
-
-    lax.fori_loop(1, F * T, share_start, 0)
-    lax.fori_loop(1, F * T, share_wait, 0)
-    total = jnp.sum(tot_in[...], axis=0)
+    tot_two[...] = jnp.sum(tot_in[:T], axis=0)
+    tot_in[T] = tot_two[...]
+    for d in range(1, F):
+        share_on(d).start()
+    for d in range(1, F):
+        share_on(d).wait()
+    total = jnp.sum(tot_in[T:], axis=0)
     factor = (scale * lax.rsqrt(total + 1e-06))[0:1, 0:1]
     for which, (first, second, first_to, second_to) in enumerate(
         ((m_in, v_in, nm_in, nv_in), (m_out, v_out, nm_out, nv_out))
@@ -363,7 +374,8 @@
             pltpu.VMEM((2, F, rr, cols), bf),
             pltpu.VMEM((2, F, rr, cols), bf),
             pltpu.VMEM((8, 128), f32),
-            pltpu.VMEM((F * T, 8, 128), f32),
+            pltpu.VMEM((8, 128), f32),
+            pltpu.VMEM((T + F, 8, 128), f32),
             dma((2, chunks, 2)),
             dma((8, Z, X)),
             dma((8, Z, X)),
@@ -371,8 +383,8 @@
             dma((2, Z, X)),
             dma((2, F)),
             dma((2, F)),
-            dma((F * T,)),
-            dma((F * T,)),
+            dma((T + F,)),
+            dma((T + F,)),
         ],
         compiler_params=pltpu.CompilerParams(
             collective_id=0, has_side_effects=True, vmem_limit_bytes=VMEM_LIMIT

time: 132 us -> 130 us (0.985)
  Pallas kernels: 131 us -> 129 us
    pallas_call x1, Pallas kernels: 121 us -> 118 us  [shards(): pl.pallas_call(functools.partial(exchange, (F, T, Z, X, scale)), out_shap...]
where the time goes in v2:
time: 130 us
  Pallas kernels  129 us (99%)
    pallas_call x1, Pallas kernels, shards(): pl.pallas_call(functools.partial(exchange, (F, T, Z, X, scale)), out_shap...  118 us
    pallas_call x1, Pallas kernels, shards(): pl.pallas_call(apply_step, grid=(F,), out_shape=tuple((jax.ShapeDtypeStru...  10.8 us

profile of v2, /device:TPU:0, one launch (start us, length us, event | category | flops | bytes accessed | tf_op | source)
XLA Modules:
  0.0 129.6 jit_solution(12068118023572585624)
XLA Ops:
  0.6 118.1 %exchange.1 = (bf16[2,8,256,256]{3,2,1,0:T(8,128)(2,1)}, bf16[8,256,640]{2,1,0:T(8,128)(2,1)}, bf16[8,640,256]{2,1,0:T(8,128)(2,1)}, bf16[2,8,32,640]{3,2,1,0:T(...) custom-call(bf16[2048,2048]{1,0:T(8,128)(2,1)} %h_hbm.1, ...), custom_call_target="tpu_custom_call" | custom-call | tf_op jit(solution)/shard_map/exchange/pallas_call | solution.py:356
  118.7 10.8 %apply_step.1 = (f32[256,640]{1,0:T(8,128)}, f32[256,640]{1,0:T(8,128)}, bf16[2048,640]{1,0:T(8,128)(2,1)}, f32[32,640]{1,0:T(8,128)}, f32[32,640]{1,0:T(8,128)}...) custom-call(bf16[256,256]{1,0:T(8,128)(2,1)} %basis_in.3, ...), custom_call_target="tpu_custom_call" | custom-call | tf_op jit(solution)/shard_map/apply_step/pallas_call | solution.py:411
